TPU v7x, 512 devices: a 8x2x16 block of a 8x8x16 slice. The times are simulated.
512 devices in a mesh: grp: 2 (over y), sp: 16 (over z), dp: 16 (over x, core).
Axes of the slice: x: 8, y: 2, z: 16, core: 2. Of those that a mesh axis runs over, the one named last changes fastest.
The devices are a block of a 8x8x16 slice.
Arguments:
- queries: bfloat16 [32, 2048, 16, 192], P(('grp', 'dp'), 'sp'), parts along dimension 0, may hold values from -41 to 41
- kv_latent: bfloat16 [32, 2048, 512], P(('grp', 'dp'), 'sp'), parts along dimension 0, may hold values from -6 to 6
- rope_key: bfloat16 [32, 2048, 64], P(('grp', 'dp'), 'sp'), parts along dimension 0, may hold values from -5.1 to 5.1
- kv_gain: float32 [512], replicated, may hold values from 0.1 to 1.9
- kv_weight: bfloat16 [512, 4096], P('dp', 'sp'), may hold values from -0.25 to 0.25
- out_weight: bfloat16 [2048, 2048], P(None, 'dp'), may hold values from -1 to 1
Outputs:
- mixed: bfloat16 [32, 2048, 2048], P(('grp', 'dp'), 'sp'), parts along dimension 0
There are 2 independent parts, one for each index of `grp`. A program takes and returns all parts, laid end to end along the dimension named above; an argument that names none is the same for every part. Nothing has to cross between parts.
All inputs are finite; a program needn't handle non-finite values.
Results may differ from a plain program's by a relative error of at most 0.0075.
Values may be sent and summed in bfloat16 or wider, within the bound.
A program may use at most 64 MiB of HBM per device.

v0:
```python
import jax
import jax.numpy as jnp
from jax import lax
from jax.sharding import PartitionSpec as P

NOPE = 128
VD = 128


def sent_to_all(value, axis):
    length = lax.axis_size(axis)
    return lax.all_to_all(
        jnp.broadcast_to(value[None], (length, *value.shape)), axis, 0, 0, tiled=True
    )


def in_order(parts, dim):
    parts = jnp.moveaxis(parts, 0, dim)
    dims = parts.shape
    return parts.reshape(*dims[:dim], dims[dim] * dims[dim + 1], *dims[dim + 2 :])


def gather_directly(value, axis, dim):
    parts = sent_to_all(value, axis)
    return in_order(parts, dim)


def rotate(values, positions):
    half = values.shape[-1] // 2
    inverse = jnp.power(10000.0, -jnp.arange(half, dtype=jnp.float32) * 2.0 / values.shape[-1])
    angle = positions.astype(jnp.float32)[..., None] * inverse
    first = values[..., :half].astype(jnp.float32)
    second = values[..., half:].astype(jnp.float32)
    cosine = jnp.cos(angle)
    sine = jnp.sin(angle)
    return jnp.concatenate(
        [first * cosine - second * sine, first * sine + second * cosine], axis=-1
    )


def attend(query_rot, key_value, key_rot):
    length, heads = (query_rot.shape[0], query_rot.shape[1])
    nope = query_rot.shape[2] - key_rot.shape[1]
    scale = query_rot.shape[2] ** (-0.5)
    content = key_value[:, :, :nope]
    values = key_value[:, :, nope:]
    shared = key_rot[:, None, :]
    keys = jnp.concatenate([content, shared], axis=-1)
    block = min(512, length)
    blocks = query_rot.reshape(length // block, block, heads, query_rot.shape[2])
    key_pos = jnp.arange(length, dtype=jnp.int32)

    def one_block(item):
        query_block, index = item
        scores = (
            jnp.einsum("qhd,khd->hqk", query_block, keys, preferred_element_type=jnp.float32)
            * scale
        )
        query_pos = index * block + jnp.arange(block, dtype=jnp.int32)
        kept = query_pos[:, None] >= key_pos[None, :]
        scores = jnp.where(kept[None], scores, -jnp.inf)
        top = jnp.max(scores, axis=-1, keepdims=True)
        expo = jnp.exp(scores - top)
        probs = (expo / jnp.sum(expo, axis=-1, keepdims=True)).astype(jnp.bfloat16)
        return jnp.einsum("hqk,khd->qhd", probs, values, preferred_element_type=jnp.float32).astype(
            jnp.bfloat16
        )

    result = lax.map(one_block, (blocks, jnp.arange(length // block, dtype=jnp.int32)))
    return result.reshape(length, heads, values.shape[2])


def body(queries, kv_latent, rope_key, kv_gain, kv_weight, out_weight):
    tok_rows = queries.shape[1]
    positions = lax.axis_index("sp") * tok_rows + jnp.arange(tok_rows, dtype=jnp.int32)
    latent32 = kv_latent[0].astype(jnp.float32)
    latent_n = (
        latent32
        * lax.rsqrt(jnp.mean(latent32 * latent32, axis=-1, keepdims=True) + 1e-06)
        * kv_gain
    ).astype(jnp.bfloat16)
    key_rot = rotate(rope_key[0], positions).astype(jnp.bfloat16)
    turned = rotate(queries[0, :, :, NOPE:], positions[:, None])
    query_rot = jnp.concatenate(
        [queries[0, :, :, :NOPE].astype(jnp.float32), turned], axis=-1
    ).astype(jnp.bfloat16)
    query_heads = lax.all_to_all(query_rot[None], "sp", split_axis=2, concat_axis=1, tiled=True)
    every_latent, every_key = (
        lax.all_gather(latent_n[None], "sp", axis=1, tiled=True),
        lax.all_gather(key_rot[None], "sp", axis=1, tiled=True),
    )
    whole_latent = every_latent[0]
    kv_heads = jnp.dot(
        whole_latent, gather_directly(kv_weight, "dp", 0), preferred_element_type=jnp.float32
    ).astype(jnp.bfloat16)
    kv_heads = kv_heads.reshape(whole_latent.shape[0], kv_weight.shape[1] // (NOPE + VD), NOPE + VD)
    attended = attend(query_heads[0], kv_heads, every_key[0])
    returned = lax.all_to_all(attended[None], "sp", split_axis=1, concat_axis=2, tiled=True)
    flat_rows = returned.reshape(tok_rows, returned.shape[2] * returned.shape[3])
    mixed = jnp.dot(
        flat_rows,
        lax.all_gather(out_weight, "dp", axis=1, tiled=True),
        preferred_element_type=jnp.float32,
    ).astype(jnp.bfloat16)
    return mixed[None]


def solution(mesh):
    return jax.shard_map(
        body,
        mesh=mesh,
        in_specs=(
            P(("grp", "dp"), "sp", None, None),
            P(("grp", "dp"), "sp", None),
            P(("grp", "dp"), "sp", None),
            P(),
            P("dp", "sp"),
            P(None, "dp"),
        ),
        out_specs=P(("grp", "dp"), "sp", None),
        check_vma=False,
    )
```

profile of v0, /device:TPU:84, one launch (start us, length us, event | category | flops | bytes accessed | tf_op | source)
XLA Modules:
  0.0 228.3 jit_solution(14194798245144524070)
XLA Ops:
  6.6 1.0 fusion.19
  7.6 1.7 fusion.21
  9.4 0.7 all-gather.5.cloned.1.call-update
  10.1 1.1 slice.32
  11.3 0.9 fusion.29
  12.1 1.0 slice_bitcast_fusion
  13.3 91.7 %all_to_all.35 = bf16[1,128,16,192]{1,3,0,2:T(8,128)(2,1)S(1)} all-to-all(bf16[1,128,16,192]{1,3,0,2:T(8,128)(2,1)S(1)} %pad_maximum_fusion), channel_id=1, replica_groups=mesh['grp'=2,'sp'=16,'dp'=16] {'sp'}, dimensions={2} | all-to-all | bytes 1572864 | tf_op jit(solution)/shard_map/all_to_all | solution.py:87
  104.9 0.7 broadcast_in_dim.13
  105.7 7.8 %all-to-all-start.1 = ((bf16[16,32,256]{2,1,0:T(8,128)(2,1)}), bf16[16,32,256]{2,1,0:T(8,128)(2,1)S(1)}, u32[]{:S(2)}, u32[]{:S(2)}) async-start(bf16[16,32,256]{2,1,0:T(8,128)(2,1)} %broadcast_in_dim.13), calls=%async_computation.1 | async-start | bytes 524288 | tf_op jit(solution)/shard_map/all_to_all | solution.py:12
  113.5 32.2 %all_gather.10 = bf16[1,2048,64]{1,2,0:T(8,128)(2,1)S(1)} all-gather(bf16[1,128,64]{1,2,0:T(8,128)(2,1)S(1)} %pad_maximum_fusion.2), channel_id=1, replica_groups=mesh['grp'=2,'sp'=16,'dp'=16] {'sp'}, dimensions={1}, use_global_device_ids=true | all-gather | bytes 278528 | tf_op jit(solution)/shard_map/all_gather | solution.py:90
  146.7 2.3 %fusion.12 = bf16[2048,1,256]{0,2,1:T(8,128)(2,1)S(1)} fusion(bf16[512,256]{1,0:T(8,128)(2,1)S(1)} %bitcast.82, bf16[1,2048,512]{2,1,0:T(8,128)(2,1)} %all-gather.3.cloned.1.call-done), kind=kOutput, calls=%fused_computation.17 | convolution fusion | flops 537395200 | bytes 3407872 | tf_op jit(solution)/shard_map/dot_general | solution.py:93
  149.1 1.0 copy.27
  150.2 16.9 %while.11 = (s32[]{:T(128)}, bf16[4,512,1,128]{3,1,2,0:T(8,128)(2,1)S(1)}, s32[4]{0:T(128)S(1)}, bf16[4,512,1,192]{1,3,2,0:T(8,128)(2,1)S(1)}, bf16[2048,1,192]{...) while((s32[]{:T(128)}, ...), condition=%wide.region_4.5_spmd.clone, body=%wide.region_1.4_spmd.clone.sunk | while | flops 680590848 | bytes 16332949 | solution.py:69
  150.4 0.6 dynamic_slice.19
  151.5 1.0 fusion.40
  152.5 0.7 fusion.41
  153.7 0.9 fusion.42
  154.6 0.6 dynamic_slice.19
  155.8 1.0 fusion.40
  156.8 0.7 fusion.41
  157.8 0.9 fusion.42
  158.8 0.6 dynamic_slice.19
  159.9 1.0 fusion.40
  160.9 0.7 fusion.41
  162.0 0.9 fusion.42
  164.1 1.0 fusion.40
  165.1 0.7 fusion.41
  166.1 0.9 fusion.42
  167.1 8.1 %copy.32 = bf16[1,2048,1,128]{3,2,0,1:T(2,128)(2,1)S(1)} copy(bf16[1,2048,1,128]{3,1,2,0:T(8,128)(2,1)S(1)} %bitcast.84) | data formatting | bytes 1048576 | tf_op jit(solution)/shard_map/broadcast_in_dim;reshape | solution.py:98
  175.7 11.5 %reduce.5 = bf16[2048,128]{1,0:T(8,128)(2,1)S(1)} reduce(bf16[2048,1,1,128]{3,2,1,0:T(2,128)(2,1)S(1)} %bitcast.78, bf16[]{:T(256)} %broadcast.105), dimensions={1,2}, to_apply=%bitcast.65.reduce_sub_computation | reduce | bytes 1048578
  187.4 27.7 %all_to_all.36 = bf16[16,2,8192]{2,1,0:T(2,128)(2,1)S(1)} all-to-all(bf16[16,2,8192]{2,1,0:T(2,128)(2,1)S(1)} %reshape.234), channel_id=1, replica_groups=mesh['grp'=2,'sp'=16,'dp'=16] {'sp'}, dimensions={0} | all-to-all | bytes 1048576 | tf_op jit(solution)/shard_map/all_to_all | solution.py:98
  216.0 5.5 %fusion.13 = bf16[1,128,2048]{2,1,0:T(8,128)(2,1)} fusion(bf16[128,2048]{0,1:T(8,128)(2,1)S(1)} %bitcast.76, bf16[2048,2048]{1,0:T(8,128)(2,1)} %all-gather.5.cloned.1.call-done), kind=kOutput, calls=%fused_computation.19 | convolution fusion | flops 1074003968 | bytes 9437184 | tf_op jit(solution)/shard_map/dot_general | solution.py:100
  (39 shorter events, 5.0 us)
Async XLA Ops:
  6.5 98.4 %copy-start.1 = (bf16[32,256]{1,0:T(8,128)(2,1)S(1)}, bf16[32,256]{1,0:T(8,128)(2,1)}, u32[]{:S(2)}) copy-start(bf16[32,256]{1,0:T(8,128)(2,1)} %param.12) | copy-start | bytes 49156
  6.5 140.1 %all-gather.3.cloned.1.call-start = ((), (), s32[]{:S(2)}) async-start(), calls=%async_computation.3 | async-start | bytes 2228224 | tf_op jit(solution)/shard_map/all_gather | solution.py:89
  9.3 206.7 %all-gather.5.cloned.1.call-start = ((), (), s32[]{:S(2)}) async-start(), calls=%async_computation.4 | async-start | bytes 8912896 | tf_op jit(solution)/shard_map/all_gather | solution.py:102
  105.7 41.0 %all-to-all-start.1 = ((bf16[16,32,256]{2,1,0:T(8,128)(2,1)}), bf16[16,32,256]{2,1,0:T(8,128)(2,1)S(1)}, u32[]{:S(2)}, u32[]{:S(2)}) async-start(bf16[16,32,256]{2,1,0:T(8,128)(2,1)} %broadcast_in_dim.13), calls=%async_computation.1 | async-start | bytes 524288 | tf_op jit(solution)/shard_map/all_to_all | solution.py:12
  152.5 1.2 copy-start
  156.8 1.0 copy-start
  160.9 1.1 copy-start
  165.1 1.0 copy-start
Sparse Core Ops, SparseCore 0:
  9.4 127.1 all-gather.2
  138.7 67.0 all-gather.4
where the time goes:
time: 229 us; the launch traced here: 228 us
  blocking collectives  152 us (66%)
  local copies, waits for them, and re-layouts  18.1 us (8%)
  other arithmetic  18.1 us (8%)
  matrix products  15.7 us (7%)
  between operations  13.6 us (6%)
  starting transfers between devices  7.86 us (3%)
  loops' own time  2.5 us (1%)
    all_to_all x1, blocking collectives, body(): lax.all_to_all(query_rot[None], 'sp', split_axis=2, concat_axis=1, tiled=...  91.7 us
    all_gather x1, blocking collectives, body(): lax.all_gather(key_rot[None], 'sp', axis=1, tiled=True)  32.2 us
    all_to_all x1, blocking collectives, body(): lax.all_to_all(attended[None], 'sp', split_axis=1, concat_axis=2, tiled=T...  27.7 us
    unnamed x1, other arithmetic  11.5 us
    another operation x1, local copies, waits for them, and re-layouts, body(): attended[None]  8.14 us
    all_to_all x1, starting transfers between devices, sent_to_all(): lax.all_to_all(jnp.broadcast_to(value[None], (length, *value.shape)), axi...  7.79 us
    dot_general x1, matrix products, body(): jnp.dot(flat_rows, lax.all_gather(out_weight, 'dp', axis=1, tiled=True),...  5.46 us
  transfers between devices with their start and end apart: 3, of which 0 were waited for; matrix products, arithmetic and copies ran while one was open for 19% of the time, Pallas kernels for 0%

commit v1 on v0

--- a/solution.py
+++ b/solution.py
@@ -85,9 +85,17 @@
         [queries[0, :, :, :NOPE].astype(jnp.float32), turned], axis=-1
     ).astype(jnp.bfloat16)
     query_heads = lax.all_to_all(query_rot[None], "sp", split_axis=2, concat_axis=1, tiled=True)
+
+    def _convert_cells(view, which_dim):
+        finding = jnp.concatenate(
+            lax.all_to_all(jnp.stack([view for _ in range(lax.axis_size("sp"))], 0), "sp", 0, 0),
+            which_dim,
+        )
+        return finding
+
     every_latent, every_key = (
         lax.all_gather(latent_n[None], "sp", axis=1, tiled=True),
-        lax.all_gather(key_rot[None], "sp", axis=1, tiled=True),
+        _convert_cells(key_rot[None], 1),
     )
     whole_latent = every_latent[0]
     kv_heads = jnp.dot(

time: 229 us -> 238 us (1.039)
  the two profiles are of different devices: /device:TPU:84 before, /device:TPU:80 now
where the time goes in v1:
time: 238 us
  blocking collectives  88.8 us (37%)
  starting transfers between devices  53.1 us (22%)
  waiting for transfers between devices  28.2 us (12%)
  other arithmetic  18.4 us (8%)
  local copies, waits for them, and re-layouts  17.1 us (7%)
  matrix products  15.7 us (7%)
  between operations  13.6 us (6%)
  loops' own time  2.7 us (1%)
    all_to_all x1, blocking collectives, body(): lax.all_to_all(query_rot[None], 'sp', split_axis=2, concat_axis=1, tiled=...  52.5 us
    all_to_all x1, starting transfers between devices, _convert_cells(): lax.all_to_all(jnp.stack([view for _ in range(lax.axis_size('sp'))], 0),...  43.7 us
    all_to_all x1, blocking collectives, body(): lax.all_to_all(attended[None], 'sp', split_axis=1, concat_axis=2, tiled=T...  36.4 us
    all_to_all x1, waiting for transfers between devices, _convert_cells(): lax.all_to_all(jnp.stack([view for _ in range(lax.axis_size('sp'))], 0),...  17.7 us
    unnamed x1, other arithmetic  11.7 us
    all_to_all x1, waiting for transfers between devices, sent_to_all(): lax.all_to_all(jnp.broadcast_to(value[None], (length, *value.shape)), axi...  9.65 us
    all_to_all x1, starting transfers between devices, sent_to_all(): lax.all_to_all(jnp.broadcast_to(value[None], (length, *value.shape)), axi...  9.4 us
    another operation x1, local copies, waits for them, and re-layouts, body(): attended[None]  8.14 us
  transfers between devices with their start and end apart: 4, of which 2 were waited for; matrix products, arithmetic and copies ran while one was open for 18% of the time, Pallas kernels for 0%

profile of v1, /device:TPU:80, one launch (start us, length us, event | category | flops | bytes accessed | tf_op | source)
XLA Modules:
  0.0 237.7 jit_solution(11750779639200035465)
XLA Ops:
  6.6 1.0 fusion.19
  7.6 1.7 fusion.21
  9.4 0.7 all-gather.5.cloned.1.call-update
  10.2 0.9 fusion.25
  11.0 0.8 stack.3
  11.8 43.7 %all-to-all-start.2 = ((bf16[16,1,128,64]{2,3,1,0:T(8,128)(2,1)}), bf16[16,1,128,64]{2,3,1,0:T(8,128)(2,1)S(1)}, u32[]{:S(2)}, u32[]{:S(2)}) async-start(bf16[16,1,128,64]{2,3,1,0:T(8,128)(2,1)} %stack.3), calls=%async_computation.2 | async-start | bytes 524288 | tf_op jit(solution)/shard_map/all_to_all | solution.py:91
  55.5 1.1 slice.32
  56.6 1.0 slice_bitcast_fusion
  57.7 17.7 %all-to-all-done.2 = bf16[16,1,128,64]{2,3,1,0:T(8,128)(2,1)S(1)} async-done(((bf16[16,1,128,64]{2,3,1,0:T(8,128)(2,1)}), bf16[16,1,128,64]{2,3,1,0:T(8,128)(2,1)S(1)}, u32[]{:S(2)}, u32[]{:S(2)}) %all-to-all-start.2) | async-done | bytes 262176 | tf_op jit(solution)/shard_map/all_to_all | solution.py:91
  75.4 52.5 %all_to_all.40 = bf16[1,128,16,192]{1,3,0,2:T(8,128)(2,1)S(1)} all-to-all(bf16[1,128,16,192]{1,3,0,2:T(8,128)(2,1)S(1)} %pad_maximum_fusion), channel_id=1, replica_groups=mesh['grp'=2,'sp'=16,'dp'=16] {'sp'}, dimensions={2} | all-to-all | bytes 1572864 | tf_op jit(solution)/shard_map/all_to_all | solution.py:87
  127.9 0.7 broadcast_in_dim.13
  128.6 9.4 %all-to-all-start.1 = ((bf16[16,32,256]{2,1,0:T(8,128)(2,1)}), bf16[16,32,256]{2,1,0:T(8,128)(2,1)S(1)}, u32[]{:S(2)}, u32[]{:S(2)}) async-start(bf16[16,32,256]{2,1,0:T(8,128)(2,1)} %broadcast_in_dim.13), calls=%async_computation.1 | async-start | bytes 524288 | tf_op jit(solution)/shard_map/all_to_all | solution.py:12
  139.3 9.7 %all-to-all-done.1 = bf16[16,32,256]{2,1,0:T(8,128)(2,1)S(1)} async-done(((bf16[16,32,256]{2,1,0:T(8,128)(2,1)}), bf16[16,32,256]{2,1,0:T(8,128)(2,1)S(1)}, u32[]{:S(2)}, u32[]{:S(2)}) %all-to-all-start.1) | async-done | bytes 262176 | tf_op jit(solution)/shard_map/all_to_all | solution.py:12
  149.0 2.3 fusion.12
  151.8 15.8 %while.11 = (s32[]{:T(128)}, bf16[4,512,1,128]{3,1,2,0:T(8,128)(2,1)S(1)}, s32[4]{0:T(128)S(1)}, bf16[4,512,1,192]{1,3,2,0:T(8,128)(2,1)S(1)}, bf16[2048,1,192]{...) while((s32[]{:T(128)}, ...), condition=%wide.region_4.5_spmd.clone, body=%wide.region_1.4_spmd.clone.sunk | while | flops 680590848 | bytes 14235769 | solution.py:69
  151.8 0.6 dynamic_slice.19
  153.0 1.0 fusion.38
  154.1 0.7 fusion.39
  154.8 0.9 fusion.40
  157.0 1.0 fusion.38
  158.0 0.7 fusion.39
  158.7 0.9 fusion.40
  160.9 1.0 fusion.38
  162.0 0.7 fusion.39
  162.7 0.9 fusion.40
  164.9 1.0 fusion.38
  165.9 0.7 fusion.39
  166.6 0.9 fusion.40
  167.6 8.1 %copy.34 = bf16[1,2048,1,128]{3,2,0,1:T(2,128)(2,1)S(1)} copy(bf16[1,2048,1,128]{3,1,2,0:T(8,128)(2,1)S(1)} %bitcast.82) | data formatting | bytes 1048576 | tf_op jit(solution)/shard_map/broadcast_in_dim;reshape | solution.py:106
  176.2 11.7 %reduce.5 = bf16[2048,128]{1,0:T(8,128)(2,1)S(1)} reduce(bf16[2048,1,1,128]{3,2,1,0:T(2,128)(2,1)S(1)} %bitcast.77, bf16[]{:T(256)} %broadcast.107), dimensions={1,2}, to_apply=%bitcast.64.reduce_sub_computation | reduce | bytes 1048578
  188.1 36.4 %all_to_all.41 = bf16[16,2,8192]{2,1,0:T(2,128)(2,1)S(1)} all-to-all(bf16[16,2,8192]{2,1,0:T(2,128)(2,1)S(1)} %reshape.224), channel_id=1, replica_groups=mesh['grp'=2,'sp'=16,'dp'=16] {'sp'}, dimensions={0} | all-to-all | bytes 1048576 | tf_op jit(solution)/shard_map/all_to_all | solution.py:106
  225.4 5.5 %fusion.13 = bf16[1,128,2048]{2,1,0:T(8,128)(2,1)} fusion(bf16[128,2048]{0,1:T(8,128)(2,1)S(1)} %bitcast.75, bf16[2048,2048]{1,0:T(8,128)(2,1)} %all-gather.5.cloned.1.call-done), kind=kOutput, calls=%fused_computation.19 | convolution fusion | flops 1074003968 | bytes 9437184 | tf_op jit(solution)/shard_map/dot_general | solution.py:108
  (35 shorter events, 5.3 us)
Async XLA Ops:
  6.5 121.4 %copy-start = (bf16[32,256]{1,0:T(8,128)(2,1)S(1)}, bf16[32,256]{1,0:T(8,128)(2,1)}, u32[]{:S(2)}) copy-start(bf16[32,256]{1,0:T(8,128)(2,1)} %param.12) | copy-start | bytes 49156
  6.5 142.4 %all-gather.3.cloned.1.call-start = ((), (), s32[]{:S(2)}) async-start(), calls=%async_computation.4 | async-start | bytes 2228224 | tf_op jit(solution)/shard_map/all_gather | solution.py:97
  9.3 216.1 %all-gather.5.cloned.1.call-start = ((), (), s32[]{:S(2)}) async-start(), calls=%async_computation.5 | async-start | bytes 8912896 | tf_op jit(solution)/shard_map/all_gather | solution.py:110
  11.8 63.6 %all-to-all-start.2 = ((bf16[16,1,128,64]{2,3,1,0:T(8,128)(2,1)}), bf16[16,1,128,64]{2,3,1,0:T(8,128)(2,1)S(1)}, u32[]{:S(2)}, u32[]{:S(2)}) async-start(bf16[16,1,128,64]{2,3,1,0:T(8,128)(2,1)} %stack.3), calls=%async_computation.2 | async-start | bytes 524288 | tf_op jit(solution)/shard_map/all_to_all | solution.py:91
  128.6 20.3 %all-to-all-start.1 = ((bf16[16,32,256]{2,1,0:T(8,128)(2,1)}), bf16[16,32,256]{2,1,0:T(8,128)(2,1)S(1)}, u32[]{:S(2)}, u32[]{:S(2)}) async-start(bf16[16,32,256]{2,1,0:T(8,128)(2,1)} %broadcast_in_dim.13), calls=%async_computation.1 | async-start | bytes 524288 | tf_op jit(solution)/shard_map/all_to_all | solution.py:12
Sparse Core Ops, SparseCore 0:
  9.4 134.2 all-gather.2
  145.8 66.3 all-gather.4
